TPU v7x, 32 devices: a whole 2x2x4 slice. The times are simulated.
32 devices in a mesh: fs: 16 (over z, y, x), tp: 2 (over core).
Axes of the slice: x: 2, y: 2, z: 4, core: 2. Of those that a mesh axis runs over, the one named last changes fastest.
Arguments:
- fwd_input: bfloat16 [2048, 2048], P('fs'), may hold values from -6 to 6
- saved_input: bfloat16 [2048, 2048], P('fs'), may hold values from -6 to 6
- out_cotangent: bfloat16 [2048, 2048], P('fs'), may hold values from -6 to 6
- up_weight: bfloat16 [2048, 4096], P('fs', 'tp'), may hold values from -0.125 to 0.125
- down_weight: bfloat16 [4096, 2048], P('tp', 'fs'), may hold values from -0.09375 to 0.09375
- up_grad_sum: float32 [2048, 4096], P('fs', 'tp'), may hold values from -6 to 6
Outputs:
- layer_out: bfloat16 [2048, 2048], P('fs')
- input_grad: bfloat16 [2048, 2048], P('fs')
- up_grad_out: float32 [2048, 4096], P('fs', 'tp')
All inputs are finite; a program needn't handle non-finite values.
Results may differ from a plain program's by a relative error of at most 0.013.
Values may be sent and summed in bfloat16 or wider, within the bound.
A program may use at most 128 MiB of HBM per device.

v0:
```python
import jax
import jax.numpy as jnp
from jax import lax
from jax.sharding import PartitionSpec as P


def per_device(fwd_input, saved_input, out_cotangent, up_weight, down_weight, up_grad_sum):
    row_count = fwd_input.shape[0]
    stacked = jnp.concatenate([fwd_input, saved_input], axis=0)
    up_whole = lax.all_gather(up_weight, "fs", axis=0, tiled=True)
    down_whole = lax.all_gather(down_weight, "fs", axis=1, tiled=True)
    pre_both = jnp.dot(stacked, up_whole, preferred_element_type=jnp.float32)
    pre_fwd = pre_both[:row_count]
    pre_bwd = pre_both[row_count:]
    positive = jnp.maximum(pre_fwd, 0.0)
    hidden = (positive * positive).astype(jnp.bfloat16)
    out_part = jnp.dot(hidden, down_whole, preferred_element_type=jnp.float32)
    layer_out = lax.psum(out_part.astype(jnp.bfloat16), "tp")
    d_hidden = lax.dot_general(
        out_cotangent, down_whole, (((1,), (1,)), ((), ())), preferred_element_type=jnp.float32
    )
    d_pre = (d_hidden * 2.0 * jnp.maximum(pre_bwd, 0.0)).astype(jnp.bfloat16)
    in_part = lax.dot_general(
        d_pre, up_whole, (((1,), (1,)), ((), ())), preferred_element_type=jnp.float32
    )
    input_grad = lax.psum(in_part.astype(jnp.bfloat16), "tp")
    grad_part = lax.psum_scatter(
        lax.dot_general(
            saved_input, d_pre, (((0,), (0,)), ((), ())), preferred_element_type=jnp.float32
        ),
        "fs",
        scatter_dimension=0,
        tiled=True,
    )
    grad_scale = float(row_count * lax.axis_size("fs")) ** (-0.5)
    return (layer_out, input_grad, up_grad_sum + grad_part * grad_scale)


def solution(mesh):
    placed = (
        P("fs", None),
        P("fs", None),
        P("fs", None),
        P("fs", "tp"),
        P("tp", "fs"),
        P("fs", "tp"),
    )
    return jax.shard_map(
        per_device,
        mesh=mesh,
        in_specs=placed,
        out_specs=(P("fs", None), P("fs", None), P("fs", "tp")),
        check_vma=False,
    )
```

profile of v0, /device:TPU:0, one launch (start us, length us, event | category | flops | bytes accessed | tf_op | source)
XLA Modules:
  0.0 666.1 jit_solution(1798604370416390500)
XLA Ops:
  7.2 0.0 copy-start
  7.2 0.0 all-gather.3.cloned.1.call-start
  7.2 0.7 all-gather.3.cloned.1.call-update
  7.9 0.0 all-gather.5.cloned.1.call-start
  8.0 0.7 all-gather.5.cloned.1.call-update
  8.7 0.0 reduce-scatter.2.cloned.1.call-start
  8.7 117.1 %all-gather.3.cloned.1.call-done = bf16[2048,2048]{1,0:T(8,128)(2,1)} async-done(((bf16[128,2048]{1,0:T(8,128)(2,1)}), bf16[2048,2048]{1,0:T(8,128)(2,1)}) %all-gather.3.cloned.1.call-update) | async-done | bytes 8388624 | tf_op jit(solution)/shard_map/all_gather | solution.py:10
  125.8 6.0 fusion.4
  131.9 136.7 %all-gather.5.cloned.1.call-done = bf16[2048,2048]{1,0:T(8,128)(2,1)} async-done(((bf16[2048,128]{1,0:T(8,128)(2,1)}), bf16[2048,2048]{1,0:T(8,128)(2,1)}) %all-gather.5.cloned.1.call-update) | async-done | bytes 8388624 | tf_op jit(solution)/shard_map/all_gather | solution.py:11
  268.6 0.0 copy-done
  268.6 0.0 copy-start.1
  268.6 6.3 fusion.1
  274.9 0.0 copy-done.1
  274.9 8.1 %convolution_bitcast_fusion = f32[2048,2048]{0,1:T(8,128)} fusion(bf16[128,2048]{1,0:T(8,128)(2,1)S(1)} %fusion.1, bf16[128,2048]{1,0:T(8,128)(2,1)S(1)} %copy-done.1), kind=kOutput, calls=%fused_computation | convolution fusion | flops 1073741824 | bytes 17825792 | tf_op jit(solution)/shard_map/dot_general | solution.py:28
  283.0 0.0 reduce-scatter.2.cloned.1.call-update
  283.0 0.0 all-reduce.3.cloned.1.call-start
  283.1 7.1 %convolution_convert_fusion = bf16[128,2048]{1,0:T(8,128)(2,1)} fusion(bf16[128,2048]{1,0:T(8,128)(2,1)S(1)} %fusion.1, bf16[2048,2048]{1,0:T(8,128)(2,1)} %all-gather.3.cloned.1.call-done), kind=kOutput, calls=%fused_computation.3 | convolution fusion | flops 1074003968 | bytes 9437184 | tf_op jit(solution)/shard_map/dot_general | solution.py:23
  290.2 5.4 convolution_convert_fusion.1
  295.6 0.0 all-reduce.3.cloned.1.call-update
  295.6 1.6 copy.9
  297.2 330.6 %reduce-scatter.2.cloned.1.call-done = f32[128,2048]{0,1:T(8,128)} async-done(((f32[2048,2048]{0,1:T(8,128)}), f32[128,2048]{0,1:T(8,128)}) %reduce-scatter.2.cloned.1.call-update) | async-done | bytes 1048592 | tf_op jit(solution)/shard_map/reduce_scatter | solution.py:27
  627.8 1.3 multiply_add_fusion
  629.2 1.3 copy.10
  630.5 25.3 %all-reduce.3.cloned.1.call-done = (bf16[128,2048]{1,0:T(8,128)(2,1)}, bf16[128,2048]{1,0:T(8,128)(2,1)}) async-done(((bf16[128,2048]{1,0:T(8,128)(2,1)}, bf16[128,2048]{1,0:T(8,128)(2,1)}), (bf16[128,2048]{1,0:T(8,128)(2,1)}, bf16[128,2048]{1,0:T(8,128)(2,1)})) %all-reduce.3.cloned.1.call-update) | async-done | bytes 1048592 | tf_op jit(solution)/shard_map/psum | solution.py:18
  655.8 1.9 copy.13
  657.7 1.9 copy.14
Async XLA Ops:
  7.2 261.4 %copy-start = (bf16[128,2048]{1,0:T(8,128)(2,1)S(1)}, bf16[128,2048]{1,0:T(8,128)(2,1)}, u32[]{:S(2)}) copy-start(bf16[128,2048]{1,0:T(8,128)(2,1)} %param.8) | copy-start | bytes 1572868
  7.2 118.6 %all-gather.3.cloned.1.call-start = ((), (), s32[]{:S(2)}) async-start(), calls=%async_computation.1 | async-start | bytes 8912896 | tf_op jit(solution)/shard_map/all_gather | solution.py:10
  7.9 260.6 %all-gather.5.cloned.1.call-start = ((), (), s32[]{:S(2)}) async-start(), calls=%async_computation.2 | async-start | bytes 8912896 | tf_op jit(solution)/shard_map/all_gather | solution.py:11
  8.7 619.1 %reduce-scatter.2.cloned.1.call-start = ((), (), s32[]{:S(2)}) async-start(), calls=%async_computation.3 | async-start | bytes 17825792 | tf_op jit(solution)/shard_map/reduce_scatter | solution.py:27
  268.6 6.3 copy-start.1
  283.0 372.7 %all-reduce.3.cloned.1.call-start = ((), (), s32[]{:S(2)}) async-start(), calls=%async_computation.4 | async-start | bytes 2097152 | tf_op jit(solution)/shard_map/psum | solution.py:18
Sparse Core Ops, SparseCore 0:
  10.8 115.0 all-gather.2
  128.5 139.9 all-gather.4
  283.2 344.5 reduce-scatter.1
  630.6 25.1 all-reduce.2
where the time goes:
time: 666 us
  waiting for transfers between devices  611 us (92%)
  matrix products  33 us (5%)
  between operations  13.8 us (2%)
    reduce_scatter x1, waiting for transfers between devices, per_device(): lax.psum_scatter(lax.dot_general(saved_input, d_pre, (((0,), (0,)), ((),...  331 us
    all_gather x1, waiting for transfers between devices, per_device(): down_whole = lax.all_gather(down_weight, 'fs', axis=1, tiled=True)  137 us
    all_gather x1, waiting for transfers between devices, per_device(): up_whole = lax.all_gather(up_weight, 'fs', axis=0, tiled=True)  117 us
    psum x1, waiting for transfers between devices, per_device(): layer_out = lax.psum(out_part.astype(jnp.bfloat16), 'tp')  25.3 us
  transfers between devices with their start and end apart: 4, of which 4 were waited for; matrix products, arithmetic and copies ran while one was open for 3% of the time, Pallas kernels for 0%

commit v1 on v0

--- a/solution.py
+++ b/solution.py
@@ -8,7 +8,14 @@
     row_count = fwd_input.shape[0]
     stacked = jnp.concatenate([fwd_input, saved_input], axis=0)
     up_whole = lax.all_gather(up_weight, "fs", axis=0, tiled=True)
-    down_whole = lax.all_gather(down_weight, "fs", axis=1, tiled=True)
+
+    def resolve_the_rails(raw):
+        seen = []
+        for _ in range(lax.axis_size("fs")):
+            seen.append(raw)
+        return jnp.concatenate(lax.all_to_all(jnp.stack(seen), "fs", 0, 0), axis=1)
+
+    down_whole = resolve_the_rails(down_weight)
     pre_both = jnp.dot(stacked, up_whole, preferred_element_type=jnp.float32)
     pre_fwd = pre_both[:row_count]
     pre_bwd = pre_both[row_count:]

time: 666 us -> 687 us (1.032)
  starting transfers between devices: 0.16 us -> 8.65 us
  waiting for transfers between devices: 611 us -> 618 us
    all_gather x1 -> x0, waiting for transfers between devices: 137 us -> none  [per_device(): down_whole = lax.all_gather(down_weight, 'fs', axis=1, tiled=True)]
    all_gather x1, waiting for transfers between devices: 117 us -> 243 us  [per_device(): up_whole = lax.all_gather(up_weight, 'fs', axis=0, tiled=True)]
    reduce_scatter x1, waiting for transfers between devices: 331 us -> 348 us  [per_device(): lax.psum_scatter(lax.dot_general(saved_input, d_pre, (((0,), (0,)), ((),...]
    all_to_all x0 -> x1, starting transfers between devices: none -> 8.52 us  [resolve_the_rails(): return jnp.concatenate(lax.all_to_all(jnp.stack(seen), 'fs', 0, 0), axis=1)]
  transfers between devices with their start and end apart: 4 -> 4, of which waited for: 4 -> 3; matrix products, arithmetic and copies ran while one was open for 3% -> 4% of each run, Pallas kernels for 0% -> 0%
where the time goes in v1:
time: 687 us
  waiting for transfers between devices  618 us (90%)
  matrix products  32.9 us (5%)
  between operations  13.8 us (2%)
  local copies, waits for them, and re-layouts  12.2 us (2%)
  starting transfers between devices  8.65 us (1%)
    reduce_scatter x1, waiting for transfers between devices, per_device(): lax.psum_scatter(lax.dot_general(saved_input, d_pre, (((0,), (0,)), ((),...  348 us
    all_gather x1, waiting for transfers between devices, per_device(): up_whole = lax.all_gather(up_weight, 'fs', axis=0, tiled=True)  243 us
    psum x1, waiting for transfers between devices, per_device(): layer_out = lax.psum(out_part.astype(jnp.bfloat16), 'tp')  25.5 us
  transfers between devices with their start and end apart: 4, of which 3 were waited for; matrix products, arithmetic and copies ran while one was open for 4% of the time, Pallas kernels for 0%

profile of v1, /device:TPU:0, one launch (start us, length us, event | category | flops | bytes accessed | tf_op | source)
XLA Modules:
  0.0 686.6 jit_solution(3622102171779442758)
XLA Ops:
  7.2 0.0 copy-start
  7.2 0.0 all-gather.2.cloned.1.call-start
  7.2 0.7 all-gather.2.cloned.1.call-update
  7.9 1.2 copy.11
  9.2 4.3 stack.2
  13.5 0.0 copy-start.1
  13.5 8.5 %all-to-all-start = ((bf16[16,2048,128]{1,2,0:T(8,128)(2,1)}), bf16[16,2048,128]{1,2,0:T(8,128)(2,1)}, u32[]{:S(2)}, u32[]{:S(2)}) async-start(bf16[16,2048,128]{1,2,0:T(8,128)(2,1)} %stack.2), calls=%async_computation | async-start | bytes 16777216 | tf_op jit(solution)/shard_map/all_to_all | solution.py:16
  22.0 0.0 reduce-scatter.2.cloned.1.call-start
  22.1 243.3 %all-gather.2.cloned.1.call-done = bf16[2048,2048]{1,0:T(8,128)(2,1)} async-done(((bf16[128,2048]{1,0:T(8,128)(2,1)}), bf16[2048,2048]{1,0:T(8,128)(2,1)}) %all-gather.2.cloned.1.call-update) | async-done | bytes 8388624 | tf_op jit(solution)/shard_map/all_gather | solution.py:10
  265.4 0.0 copy-done.1
  265.4 5.9 fusion.4
  271.3 0.0 all-to-all-done
  271.3 0.0 copy-start.2
  271.3 0.0 copy-done
  271.3 4.8 fusion.1
  276.1 0.0 copy-done.2
  276.1 8.1 %convolution_bitcast_fusion = f32[2048,2048]{0,1:T(8,128)} fusion(bf16[128,2048]{1,0:T(8,128)(2,1)S(1)} %fusion.1, bf16[128,2048]{1,0:T(8,128)(2,1)S(1)} %copy-done.2), kind=kOutput, calls=%fused_computation | convolution fusion | flops 1073741824 | bytes 17825792 | tf_op jit(solution)/shard_map/dot_general | solution.py:35
  284.2 0.0 reduce-scatter.2.cloned.1.call-update
  284.2 0.0 all-reduce.3.cloned.1.call-start
  284.3 7.1 %convolution_convert_fusion = bf16[128,2048]{1,0:T(8,128)(2,1)} fusion(bf16[128,2048]{1,0:T(8,128)(2,1)S(1)} %fusion.1, bf16[2048,2048]{1,0:T(8,128)(2,1)} %all-gather.2.cloned.1.call-done), kind=kOutput, calls=%fused_computation.3 | convolution fusion | flops 1074003968 | bytes 9437184 | tf_op jit(solution)/shard_map/dot_general | solution.py:30
  291.3 7.1 %convolution_convert_fusion.1 = bf16[128,2048]{1,0:T(8,128)(2,1)} fusion(bf16[2048,2048]{0,1:T(8,128)(2,1)} %bitcast.1, f32[256,2048]{1,0:T(8,128)S(1)} %fusion.4), kind=kOutput, calls=%fused_computation.4 | convolution fusion | flops 1074790400 | bytes 9961472 | tf_op jit(solution)/shard_map/dot_general | solution.py:24
  298.4 0.0 all-reduce.3.cloned.1.call-update
  298.4 1.6 copy.12
  300.0 348.2 %reduce-scatter.2.cloned.1.call-done = f32[128,2048]{0,1:T(8,128)} async-done(((f32[2048,2048]{0,1:T(8,128)}), f32[128,2048]{0,1:T(8,128)}) %reduce-scatter.2.cloned.1.call-update) | async-done | bytes 1048592 | tf_op jit(solution)/shard_map/reduce_scatter | solution.py:34
  648.2 1.3 multiply_add_fusion
  649.6 1.3 copy.13
  650.9 25.5 %all-reduce.3.cloned.1.call-done = (bf16[128,2048]{1,0:T(8,128)(2,1)}, bf16[128,2048]{1,0:T(8,128)(2,1)}) async-done(((bf16[128,2048]{1,0:T(8,128)(2,1)}, bf16[128,2048]{1,0:T(8,128)(2,1)}), (bf16[128,2048]{1,0:T(8,128)(2,1)}, bf16[128,2048]{1,0:T(8,128)(2,1)})) %all-reduce.3.cloned.1.call-update) | async-done | bytes 1048592 | tf_op jit(solution)/shard_map/psum | solution.py:25
  676.3 1.9 copy.16
  678.2 1.9 copy.17
Async XLA Ops:
  7.2 264.1 %copy-start = (bf16[128,2048]{1,0:T(8,128)(2,1)S(1)}, bf16[128,2048]{1,0:T(8,128)(2,1)}, u32[]{:S(2)}) copy-start(bf16[128,2048]{1,0:T(8,128)(2,1)} %param.8) | copy-start | bytes 1572868
  7.2 258.2 %all-gather.2.cloned.1.call-start = ((), (), s32[]{:S(2)}) async-start(), calls=%async_computation.2 | async-start | bytes 8912896 | tf_op jit(solution)/shard_map/all_gather | solution.py:10
  13.5 251.9 %copy-start.1 = (bf16[128,2048]{1,0:T(8,128)(2,1)S(1)}, bf16[128,2048]{1,0:T(8,128)(2,1)}, u32[]{:S(2)}) copy-start(bf16[128,2048]{1,0:T(8,128)(2,1)} %param.7) | copy-start | bytes 1572868
  13.5 257.8 %all-to-all-start = ((bf16[16,2048,128]{1,2,0:T(8,128)(2,1)}), bf16[16,2048,128]{1,2,0:T(8,128)(2,1)}, u32[]{:S(2)}, u32[]{:S(2)}) async-start(bf16[16,2048,128]{1,2,0:T(8,128)(2,1)} %stack.2), calls=%async_computation | async-start | bytes 16777216 | tf_op jit(solution)/shard_map/all_to_all | solution.py:16
  22.0 626.2 %reduce-scatter.2.cloned.1.call-start = ((), (), s32[]{:S(2)}) async-start(), calls=%async_computation.3 | async-start | bytes 17825792 | tf_op jit(solution)/shard_map/reduce_scatter | solution.py:34
  271.3 4.8 copy-start.2
  284.2 392.1 %all-reduce.3.cloned.1.call-start = ((), (), s32[]{:S(2)}) async-start(), calls=%async_computation.4 | async-start | bytes 2097152 | tf_op jit(solution)/shard_map/psum | solution.py:25
Sparse Core Ops, SparseCore 0:
  10.8 254.5 all-gather.1
  284.3 363.8 reduce-scatter.1
  651.2 25.1 all-reduce.2
